TPU v7x, 32 devices: a whole 2x2x4 slice. The times are simulated.
32 devices in a mesh: fs: 16 (over z, y, x), tp: 2 (over core).
Axes of the slice: x: 2, y: 2, z: 4, core: 2. Of those that a mesh axis runs over, the one named last changes fastest.
Arguments:
- fwd_input: bfloat16 [2048, 2048], P('fs'), may hold values from -6 to 6
- saved_input: bfloat16 [2048, 2048], P('fs'), may hold values from -6 to 6
- out_cotangent: bfloat16 [2048, 2048], P('fs'), may hold values from -6 to 6
- up_weight: bfloat16 [2048, 4096], P('fs', 'tp'), may hold values from -0.125 to 0.125
- down_weight: bfloat16 [4096, 2048], P('tp', 'fs'), may hold values from -0.09375 to 0.09375
- up_grad_sum: float32 [2048, 4096], P('fs', 'tp'), may hold values from -6 to 6
Outputs:
- layer_out: bfloat16 [2048, 2048], P('fs')
- input_grad: bfloat16 [2048, 2048], P('fs')
- up_grad_out: float32 [2048, 4096], P('fs', 'tp')
All inputs are finite; a program needn't handle non-finite values.
Results may differ from a plain program's by a relative error of at most 0.013.
Values may be sent and summed in bfloat16 or wider, within the bound.
A program may use at most 128 MiB of HBM per device.

v0:
```python
import functools

import jax
import jax.numpy as jnp
from jax import lax
from jax.experimental import pallas as pl
from jax.experimental.pallas import tpu as pltpu
from jax.sharding import PartitionSpec as P

MESH = pl.DeviceIdType.MESH
F32 = jnp.float32
BF16 = jnp.bfloat16
PART = 256


def remote(src, dst, send_sem, recv_sem, fs, tp):
    return pltpu.make_async_remote_copy(
        src_ref=src,
        dst_ref=dst,
        send_sem=send_sem,
        recv_sem=recv_sem,
        device_id=(fs, tp),
        device_id_type=MESH,
    )


def kernel(
    n, T, B, Q, fwd, saved, cot, up, down, out, ing, gout,
    X, W, turned, H, pre, O, tp_in, S, pl_in, G, from_left, from_right,
    lsem, wS, wR, zS, zR, aS, aR, bS, bR, tS, tR, pS, pR, fS, fR, gS, gL, gR, hS, hR,
):
    A = n // B
    f, t = lax.axis_index("fs"), lax.axis_index("tp")
    z, p = lax.div(f, B), lax.rem(f, B)
    far = A - 1 - z
    rows, D = fwd.shape
    C = rows // T
    Rw, F = up.shape
    Fs = F // B
    wide = Fs // Q
    tokens = B * rows
    peers = [lax.rem(p + i, B) for i in range(1, B)]
    mates = [lax.rem(t + i, T) for i in range(1, T)]
    has_left, has_right = z > 0, z < A - 1
    stages = [(c, pc) for pc in range(2) for c in range(Q)]
    last = len(stages) - 1

    def chunk(index):
        return pl.ds(pl.multiple_of(index * C, C), C)

    def cols(index, c):
        return pl.ds(pl.multiple_of(index * Fs + c * wide, wide), wide)

    barrier = pltpu.get_barrier_semaphore()
    for q in peers:
        pl.semaphore_signal(barrier, inc=1, device_id=(z * B + q, t), device_id_type=MESH)
    for m in mates:
        pl.semaphore_signal(barrier, inc=1, device_id=(f, m), device_id_type=MESH)

    @pl.when(has_left)
    def _():
        pl.semaphore_signal(barrier, inc=1, device_id=(f - B, t), device_id_type=MESH)

    @pl.when(has_right)
    def _():
        pl.semaphore_signal(barrier, inc=1, device_id=(f + B, t), device_id_type=MESH)

    ends = lax.div(z + A - 1, A) + lax.div(far + A - 1, A)
    pl.semaphore_wait(barrier, B - 1 + T - 1 + ends)

    weights = (up, down if down.shape == up.shape else turned)

    def slice_out(c, pc, i, q):
        return remote(
            weights[pc].at[:, cols(q, c)], W.at[c, pc, f], wS.at[c, pc, i], wR.at[c, pc, p], z * B + q, t
        )

    def slice_in(c, pc, q):
        there = W.at[c, pc, z * B + q]
        return remote(there, there, wS.at[c, pc, 0], wR.at[c, pc, q], z * B + q, t)

    def line(c, pc, k, q, way, src=None):
        at = k * B + q
        block = W.at[c, pc, at] if (c, pc) == stages[0] else W.at[c, pc, pl.ds(at, B)]
        target = f + B if way == 0 else f - B
        return remote(
            block if src is None else src, block, zS.at[way, c, pc, at], zR.at[c, pc, at], target, t
        )

    def own_out(c, pc, q, way):
        src = weights[pc].at[:, cols(p, c)] if q is p and (c, pc) == stages[0] else None
        line(c, pc, z, q, way, src).start()

    def both_ways(c, pc, q):
        @pl.when(has_right)
        def _():
            own_out(c, pc, q, 0)

        @pl.when(has_left)
        def _():
            own_out(c, pc, q, 1)

    own_w = [
        pltpu.make_async_copy(weights[pc].at[:, cols(p, c)], W.at[c, pc, f], lsem.at[3 + 2 * c + pc])
        for c, pc in stages
    ]
    for c, pc in stages:
        if (c, pc) == (0, 1) and weights[1] is turned:
            turned[...] = down[...].T
        for i, q in enumerate(peers):
            slice_out(c, pc, i, q).start()
        if (c, pc) == stages[0]:
            both_ways(c, pc, p)
    for copy in own_w:
        copy.start()

    acts = (fwd, saved, cot)

    def act_out(j, i, q):
        return remote(acts[j].at[chunk(t)], X.at[j, p, chunk(t)], aS.at[j, i], aR.at[j, p], z * B + q, t)

    def act_in(j, q):
        there = X.at[j, q, chunk(t)]
        return remote(there, there, aS.at[j, 0], aR.at[j, q], z * B + q, t)

    own_x = [pltpu.make_async_copy(acts[j], X.at[j, p], lsem.at[j]) for j in range(3)]
    for j in (1, 2, 0):
        own_x[j].start()
        for i, q in enumerate(peers):
            act_out(j, i, q).start()

    def act_share(i, q, o, m):
        there = X.at[:, q, chunk(t)]
        return remote(there, there, bS.at[i, o], bR.at[q, t], f, m)

    def act_shared(i, q, o, m):
        there = X.at[:, q, chunk(m)]
        return remote(there, there, bS.at[i, o], bR.at[q, m], f, m)

    for q in peers:
        slice_in(0, 0, q).wait_recv()
        both_ways(0, 0, q)

    order = [p] + peers

    def gather_step(stage, s):
        c, pc = stages[stage]
        for q in order if stage == 0 else (0,):

            @pl.when(z >= s)
            def _(q=q):
                line(c, pc, z - s, q, 0).wait_recv()

                @pl.when(has_right)
                def _():
                    line(c, pc, z - s, q, 0).start()

            @pl.when(far >= s)
            def _(q=q):
                line(c, pc, z + s, q, 1).wait_recv()

                @pl.when(has_left)
                def _():
                    line(c, pc, z + s, q, 1).start()

        if stage == 0 and s == 1:
            for later in stages[1:]:
                for q in peers:
                    slice_in(*later, q).wait_recv()
            for copy in own_w:
                copy.wait()
        if stage < last:
            @pl.when(jnp.logical_and(has_right, z == s if s > 1 else z <= 1))
            def _():
                own_out(*stages[stage + 1], 0, 0)

            @pl.when(jnp.logical_and(has_left, far == s if s > 1 else far <= 1))
            def _():
                own_out(*stages[stage + 1], 0, 1)

        if stage == last - 1 and s == 1:
            for i, q in enumerate(peers):
                for j in range(3):
                    act_in(j, q).wait_recv()
                for o, m in enumerate(mates):
                    act_share(i, q, o, m).start()

    def product(c, j, pc):
        return jnp.dot(
            X[j].reshape(tokens, D), W[c, pc].reshape(D, wide), preferred_element_type=F32
        )

    def to_right(c, d):
        return remote(G.at[c, d], from_left.at[c, d], gS.at[c, d], gL.at[c, d], f + B, t)

    def to_left(c, d):
        return remote(G.at[c, d], from_right.at[c, d], gS.at[c, d], gR.at[c, d], f - B, t)

    def add_left(c, d):
        remote(from_left.at[c, d], from_left.at[c, d], gS.at[c, d], gL.at[c, d], f - B, t).wait_recv()
        G[c, d] = (G[c, d].astype(F32) + from_left[c, d].astype(F32)).astype(BF16)

    def add_right(c, d):
        remote(from_right.at[c, d], from_right.at[c, d], gS.at[c, d], gR.at[c, d], f + B, t).wait_recv()
        G[c, d] = (G[c, d].astype(F32) + from_right[c, d].astype(F32)).astype(BF16)

    def grad_out(c, i, q):
        return remote(G.at[c, z, q], gout.at[:, cols(p, c)], hS.at[c, i], hR.at[c, p], z * B + q, t)

    def sum_step(c, s):
        if s < A - 1:

            @pl.when(jnp.logical_and(has_left, z <= s))
            def _():
                add_left(c, far - s + 2 * z)
                to_right(c, far - s + 2 * z).start()

            @pl.when(jnp.logical_and(has_right, far <= s))
            def _():
                add_right(c, s - far)
                to_left(c, s - far).start()

        else:

            @pl.when(has_left)
            def _():
                add_left(c, z)

            @pl.when(has_right)
            def _():
                add_right(c, z)

            for i, q in enumerate(peers):
                grad_out(c, i, q).start()
            gout[:, cols(p, c)] = G[c, z, p]

    planes = []
    for i in range((A + 1) // 2):
        planes += [A - 1 - i] if A - 1 - i == i else [A - 1 - i, i]
    deep = B * Rw

    def backward(c):
        d_hidden = product(c, 2, 1)
        H[1, c] = (d_hidden * 2.0 * jnp.maximum(pre[c], 0.0)).astype(BF16)
        for d in planes:
            term = lax.dot_general(
                X[1, :, :, d * deep:(d + 1) * deep].reshape(tokens, deep),
                H[1, c],
                (((0,), (0,)), ((), ())),
                preferred_element_type=F32,
            )
            G[c, d] = term.astype(BF16).reshape(B, Rw, wide)
            if d > 0:

                @pl.when(z == 0)
                def _(d=d):
                    to_right(c, d).start()

            if d < A - 1:

                @pl.when(far == 0)
                def _(d=d):
                    to_left(c, d).start()

    def forward(c):
        positive = jnp.maximum(product(c, 0, 0), 0.0)
        H[0, c] = (positive * positive).astype(BF16)
        pre[c] = product(c, 1, 0)

    def columns(k):
        return pl.ds(pl.multiple_of(k * deep, deep), deep)

    def tp_out(o, i, m, k):
        return remote(
            O.at[o, :, chunk(m), columns(k)], tp_in.at[o, t, :, :, columns(k)],
            tS.at[o, i, k], tR.at[o, t, k], f, m,
        )

    def tp_got(o, i, m, k):
        there = tp_in.at[o, m, :, :, columns(k)]
        return remote(there, there, tS.at[o, i, k], tR.at[o, m, k], f, m)

    def plane_out(o, i, q, k):
        return remote(
            S.at[o, q, :, columns(k)], pl_in.at[o, p, :, columns(k)],
            pS.at[o, i, k], pR.at[o, p, k], z * B + q, t,
        )

    def plane_got(o, i, q, k):
        there = pl_in.at[o, q, :, columns(k)]
        return remote(there, there, pS.at[o, i, k], pR.at[o, q, k], z * B + q, t)

    def spread(o, pc, k):
        part = 0.0
        for c in range(Q):
            block = W[c, pc, pl.ds(k * B, B)].reshape(deep, wide)
            part += lax.dot_general(
                H[o, c], block, (((1,), (1,)), ((), ())), preferred_element_type=F32
            )
        O[o, :, :, columns(k)] = part.astype(BF16).reshape(B, rows, deep)
        for i, m in enumerate(mates):
            tp_out(o, i, m, k).start()

    def plane_sums(o, k):
        for i, m in enumerate(mates):
            tp_got(o, i, m, k).wait_recv()
        for i, q in enumerate(peers + [p]):
            total = O[o, q, chunk(t), columns(k)].astype(F32)
            for m in mates:
                total = total + tp_in[o, m, q, :, columns(k)].astype(F32)
            S[o, q, :, columns(k)] = total.astype(BF16)
            if i < len(peers):
                plane_out(o, i, q, k).start()

    def out_step(s, work):
        if s == 0:
            work(z)
            return

        @pl.when(z >= s)
        def _():
            work(z - s)

        @pl.when(far >= s)
        def _():
            work(z + s)

    for stage in range(last + 1):
        c = stage - Q
        for s in range(1, A):
            if stage == last:
                out_step(s - 1, lambda k: spread(0, 1, k))
            gather_step(stage, s)
            if c > 0:
                sum_step(c - 1, s)
            if stage == last:
                out_step(s - 1, lambda k: plane_sums(0, k))
        if stage == last - 1:
            for copy in own_x:
                copy.wait()
            for i, q in enumerate(peers):
                for o, m in enumerate(mates):
                    act_shared(i, q, o, m).wait_recv()
            for part in range(Q):
                forward(part)
        if c >= 0:
            backward(c)

    spread(1, 0, 0)
    for k in range(1, A):
        spread(1, 0, k)
        plane_sums(1, k - 1)
    out_step(A - 1, lambda k: spread(0, 1, k))
    plane_sums(1, A - 1)
    sum_step(Q - 1, 1)
    out_step(A - 1, lambda k: plane_sums(0, k))
    for s in range(2, A):
        sum_step(Q - 1, s)

    outs = (out, ing)

    def share(o, i, m):
        there = outs[o].at[chunk(t)]
        return remote(there, there, fS.at[o, i], fR.at[o, t], f, m)

    def shared(o, i, m):
        there = outs[o].at[chunk(m)]
        return remote(there, there, fS.at[o, i], fR.at[o, m], f, m)

    for o in (0, 1):
        total = S[o, p].astype(F32)
        for i, q in enumerate(peers):
            for k in range(A):
                plane_got(o, i, q, k).wait_recv()
            total = total + pl_in[o, q].astype(F32)
        outs[o][chunk(t)] = total.astype(BF16)
        for i, m in enumerate(mates):
            share(o, i, m).start()

    for i, q in enumerate(peers):
        for c in range(Q):
            there = gout.at[:, cols(q, c)]
            remote(there, there, hS.at[c, i], hR.at[c, q], z * B + q, t).wait_recv()
            grad_out(c, i, q).wait_send()
            for pc in range(2):
                slice_out(c, pc, i, q).wait_send()
        for j in range(3):
            act_out(j, i, q).wait_send()
        for o, m in enumerate(mates):
            act_share(i, q, o, m).wait_send()
        for o in range(2):
            for k in range(A):
                plane_out(o, i, q, k).wait_send()
    for i, m in enumerate(mates):
        for o in range(2):
            for k in range(A):
                tp_out(o, i, m, k).wait_send()
            share(o, i, m).wait_send()
            shared(o, i, m).wait_recv()
    for s in range(A):

        @pl.when(jnp.logical_and(has_right, z >= s))
        def _(s=s):
            for c in range(Q):
                for pc in range(2):
                    for q in range(B if (c, pc) == stages[0] else 1):
                        line(c, pc, z - s, q, 0).wait_send()

        @pl.when(jnp.logical_and(has_left, far >= s))
        def _(s=s):
            for c in range(Q):
                for pc in range(2):
                    for q in range(B if (c, pc) == stages[0] else 1):
                        line(c, pc, z + s, q, 1).wait_send()

    for d in range(A):
        for c in range(Q):

            @pl.when(z < d)
            def _(c=c, d=d):
                to_right(c, d).wait_send()

            @pl.when(z > d)
            def _(c=c, d=d):
                to_left(c, d).wait_send()


def groups(n, width):
    size = 1
    while 4 * size * size <= n and n % (2 * size) == 0 and width // (2 * size) >= 128:
        size *= 2
    return size


def per_device(n, T, fwd_input, saved_input, out_cotangent, up_weight, down_weight, up_grad_sum):
    rows, D = fwd_input.shape
    Rw, F = up_weight.shape
    B = groups(n, F)
    A, Fs, C = n // B, F // B, rows // T
    Q = max(1, Fs // PART)
    wide = Fs // Q
    down = down_weight if Rw % 128 == 0 and down_weight.shape != up_weight.shape else down_weight.T
    dma = pltpu.SemaphoreType.DMA
    side, mate = max(B - 1, 1), max(T - 1, 1)
    flops = 12 * B * rows * Fs * D
    vmem = pl.BlockSpec(memory_space=pltpu.VMEM)
    layer_out, input_grad, grad = pl.pallas_call(
        functools.partial(kernel, n, T, B, Q),
        out_shape=(
            jax.ShapeDtypeStruct((rows, D), BF16),
            jax.ShapeDtypeStruct((rows, D), BF16),
            jax.ShapeDtypeStruct((Rw, F), BF16),
        ),
        in_specs=[vmem] * 5,
        out_specs=(vmem,) * 3,
        scratch_shapes=[
            pltpu.VMEM((3, B, rows, D), BF16),
            pltpu.VMEM((Q, 2, n, Rw, wide), BF16),
            pltpu.VMEM((Rw, F), BF16),
            pltpu.VMEM((2, Q, B * rows, wide), BF16),
            pltpu.VMEM((Q, B * rows, wide), F32),
            pltpu.VMEM((2, B, rows, D), BF16),
            pltpu.VMEM((2, T, B, C, D), BF16),
            pltpu.VMEM((2, B, C, D), BF16),
            pltpu.VMEM((2, B, C, D), BF16),
            pltpu.VMEM((Q, A, B, Rw, wide), BF16),
            pltpu.VMEM((Q, A, B, Rw, wide), BF16),
            pltpu.VMEM((Q, A, B, Rw, wide), BF16),
            dma((3 + 2 * Q,)),
            dma((Q, 2, side)), dma((Q, 2, B)),
            dma((2, Q, 2, n)), dma((Q, 2, n)),
            dma((3, side)), dma((3, B)),
            dma((side, mate)), dma((B, T)),
            dma((2, mate, A)), dma((2, T, A)),
            dma((2, side, A)), dma((2, B, A)),
            dma((2, mate)), dma((2, T)),
            dma((Q, A)), dma((Q, A)), dma((Q, A)),
            dma((Q, side)), dma((Q, B)),
        ],
        compiler_params=pltpu.CompilerParams(
            collective_id=0, has_side_effects=True, vmem_limit_bytes=58 * 2**20
        ),
        cost_estimate=pl.CostEstimate(flops=flops, bytes_accessed=2**25, transcendentals=0),
    )(fwd_input, saved_input, out_cotangent, up_weight, down)
    grad_part = grad.astype(F32)
    grad_scale = float(rows * n) ** (-0.5)
    return (layer_out, input_grad, up_grad_sum + grad_part * grad_scale)


def solution(mesh):
    placed = (
        P("fs", None),
        P("fs", None),
        P("fs", None),
        P("fs", "tp"),
        P("tp", "fs"),
        P("fs", "tp"),
    )
    return jax.shard_map(
        functools.partial(per_device, mesh.shape["fs"], mesh.shape["tp"]),
        mesh=mesh,
        in_specs=placed,
        out_specs=(P("fs", None), P("fs", None), P("fs", "tp")),
        check_vma=False,
    )
```

profile of v0, /device:TPU:0, one launch (start us, length us, event | category | flops | bytes accessed | tf_op | source)
XLA Modules:
  0.0 121.2 jit_solution(15751235714993204141)
XLA Ops:
  0.6 0.0 copy-start
  0.6 116.3 %shard_map.85 = (bf16[128,2048]{1,0:T(8,128)(2,1)}, bf16[128,2048]{1,0:T(8,128)(2,1)}, bf16[128,2048]{1,0:T(8,128)(2,1)}) custom-call(bf16[128,2048]{1,0:T(8,128)(2,1)} %fwd.1, bf16[128,2048]{1,0:T(8,128)(2,1)} %saved.1, bf16[128,2048]{1,0:T(8,128)(2,1)} %cot.1, bf16[128,2048]{1,0:T(8,128)(2,1)} %up.1, bf16[2048,128]{1,0:T(8,128)(2,1)} %down.1), custom_call_target="tpu_custom_call" | custom-call | flops 6442450944 | bytes 33554432 | tf_op jit(solution)/shard_map/pallas_call | solution.py:447
  116.9 0.0 copy-done
  117.0 0.0 copy-start.2
  117.0 2.2 %multiply_add_fusion = f32[128,2048]{1,0:T(8,128)} fusion(f32[128,2048]{1,0:T(8,128)S(1)} %copy-done, bf16[128,2048]{1,0:T(8,128)(2,1)} %get-tuple-element.8), kind=kLoop, calls=%fused_computation | loop fusion | flops 786432 | bytes 2621440 | tf_op jit(solution)/shard_map/add | solution.py:487
  119.2 0.0 copy-done.2
  119.2 0.0 copy-start.1
  119.2 0.8 copy.11
  120.0 0.4 copy-done.1
  120.4 0.8 copy.12
Async XLA Ops:
  0.6 116.3 %copy-start = (f32[128,2048]{1,0:T(8,128)S(1)}, f32[128,2048]{1,0:T(8,128)}, u32[]{:S(2)}) copy-start(f32[128,2048]{1,0:T(8,128)} %param.11) | copy-start | bytes 3145732
  117.0 2.2 %copy-start.2 = (bf16[128,2048]{1,0:T(8,128)(2,1)S(1)}, bf16[128,2048]{1,0:T(8,128)(2,1)}, u32[]{:S(2)}) copy-start(bf16[128,2048]{1,0:T(8,128)(2,1)} %get-tuple-element.12) | copy-start | bytes 1572868
  119.2 1.2 %copy-start.1 = (bf16[128,2048]{1,0:T(8,128)(2,1)S(1)}, bf16[128,2048]{1,0:T(8,128)(2,1)}, u32[]{:S(2)}) copy-start(bf16[128,2048]{1,0:T(8,128)(2,1)} %get-tuple-element.13) | copy-start | bytes 1572868
where the time goes:
time: 123 us; the launch traced here: 121 us
  Pallas kernels  116 us (94%)
  other arithmetic  2.2 us (2%)
  local copies, waits for them, and re-layouts  2.03 us (2%)
    pallas_call x1, Pallas kernels, per_device(): pl.pallas_call(functools.partial(kernel, n, T, B, Q), out_shape=(jax.Shap...  116 us

commit v1 on v0

v1 whole, which is shorter than its diff:
```python
import functools

import jax
import jax.numpy as jnp
from jax import lax
from jax.experimental import pallas as pl
from jax.experimental.pallas import tpu as pltpu
from jax.sharding import PartitionSpec as P

MESH = pl.DeviceIdType.MESH
F32 = jnp.float32
BF16 = jnp.bfloat16
PARTS = [256, 128, 128]
SCHEDULE = [('slices', 0), ('pieces', 0), ('pieces', 1), ('slices', 1), ('slices', 2), ('collect', 0, 0), ('over', 1), ('collect', 0, 1), ('relay', 0, 0, 1), ('relay', 0, 1, 1), ('near', 1), ('near', 2), ('pieces', 2), ('near', 0), ('over', 2), ('over', 0), ('take', 2, 1), ('collect', 1, 0), ('relay', 0, 0, 2), ('relay', 0, 0, 3), ('take', 1, 0), ('take', 0, 1), ('relay', 0, 1, 2), ('collect', 1, 1), ('keep_own',), ('collect', 2, 0), ('take', 1, 1), ('collect', 2, 1), ('relay', 0, 1, 3), ('relay', 1, 0, 1), ('take', 2, 0), ('take', 1, 2), ('take', 2, 2), ('settle', 1), ('settle', 2), ('take', 0, 0), ('backward', 0), ('grads', 0), ('relay', 1, 0, 2), ('relay', 2, 0, 1), ('relay', 1, 0, 3), ('relay', 1, 1, 1), ('relay', 1, 1, 2), ('take', 0, 2), ('relay', 1, 1, 3), ('settle', 0), ('backward', 1), ('grads', 1), ('forward', 0), ('forward', 1), ('relay', 2, 0, 2), ('relay', 2, 0, 3), ('forward', 2), ('relay', 2, 1, 1), ('spread_at', 0), ('spread_at', 1), ('relay', 2, 1, 2), ('tp_at', 0), ('tp_at', 1), ('spread_at', 2), ('relay', 2, 1, 3), ('backward', 2), ('tp_at', 2), ('sums', 0, 1), ('sums', 0, 2), ('spread', 1, 0), ('spread', 1, 1), ('tp_sums', 1, 0), ('grads', 2), ('spread_at', 3), ('spread', 1, 2), ('tp_at', 3), ('tp_sums', 1, 1), ('near_at', 2), ('near_at', 0), ('sums', 1, 1), ('spread', 1, 3), ('tp_sums', 1, 3), ('near_at', 1), ('tp_sums', 1, 2), ('near_sums', 1, 1), ('sums', 1, 2), ('near_at', 3), ('near_sums', 1, 2), ('near_sums', 1, 0), ('sums', 2, 1), ('sums', 0, 3), ('near_sums', 1, 3), ('sums', 1, 3), ('sums', 2, 2), ('sums', 2, 3), ('finish', 0), ('finish', 1)]


def remote(src, dst, send_sem, recv_sem, fs, tp):
    return pltpu.make_async_remote_copy(
        src_ref=src,
        dst_ref=dst,
        send_sem=send_sem,
        recv_sem=recv_sem,
        device_id=(fs, tp),
        device_id_type=MESH,
    )


def kernel(
    n, T, B, parts, fwd, saved, cot, up, down, out, ing, gout,
    X, turned, O, tp_in, S, near_in, far_in, W, H, pre, G, from_left, from_right,
    wS, wR, zS, zR, aS, aR, bS, bR, tS, tR, nS, nR, mS, mR, fS, fR,
    gS, gL, gR, hS, hR,
):
    L = n // B
    f, t = lax.axis_index("fs"), lax.axis_index("tp")
    h, p = lax.div(f, B), lax.rem(f, B)
    far = L - 1 - h
    rows, D = fwd.shape
    C = rows // T
    Rw, F = up.shape
    Fs = F // B
    Q = len(parts)
    tokens = B * rows
    deep = B * Rw
    K = D // deep
    a, b = lax.div(p, 2), lax.rem(p, 2)
    near, over, cross = 2 * a + 1 - b, 2 * (1 - a) + b, 2 * (1 - a) + 1 - b
    peers = [near, over, cross]
    mates = [lax.rem(t + i, T) for i in range(1, T)]
    has_left, has_right = h > 0, h < L - 1
    stages = [(c, pc) for c in range(Q) for pc in range(2)]

    left, right = f - B, f + B

    def dev(q):
        return h * B + q

    def chunk(index):
        return pl.ds(pl.multiple_of(index * C, C), C)

    def cols(index, c):
        return pl.ds(pl.multiple_of(index * Fs + sum(parts[:c]), 128), parts[c])

    barrier = pltpu.get_barrier_semaphore()
    for q in peers:
        pl.semaphore_signal(barrier, inc=1, device_id=(dev(q), t), device_id_type=MESH)
    for m in mates:
        pl.semaphore_signal(barrier, inc=1, device_id=(f, m), device_id_type=MESH)

    @pl.when(has_left)
    def _():
        pl.semaphore_signal(barrier, inc=1, device_id=(left, t), device_id_type=MESH)

    @pl.when(has_right)
    def _():
        pl.semaphore_signal(barrier, inc=1, device_id=(right, t), device_id_type=MESH)

    ends = lax.div(h + L - 1, L) + lax.div(far + L - 1, L)
    pl.semaphore_wait(barrier, len(peers) + T - 1 + ends)

    weights = (up, down if down.shape == up.shape else turned)

    def slice_out(c, pc, i, q):
        return remote(
            weights[pc].at[:, cols(q, c)], W[c].at[pc, h, p],
            wS.at[c, pc, i], wR.at[c, pc, p], dev(q), t,
        )

    def slice_in(c, pc, q):
        there = W[c].at[pc, h, q]
        return remote(there, there, wS.at[c, pc, 0], wR.at[c, pc, q], dev(q), t)

    def line_piece(c, pc, q, way):
        src = weights[pc].at[:, cols(p, c)] if q is p else W[c].at[pc, h, q]
        return remote(
            src, W[c].at[pc, h, q], zS.at[way, c, pc, h], zR.at[c, pc, h], right if way == 0 else left, t
        )

    def line(c, pc, k, way):
        block = W[c].at[pc, k]
        return remote(
            block, block, zS.at[way, c, pc, k], zR.at[c, pc, k], right if way == 0 else left, t
        )

    def push(c, pc, q):
        @pl.when(has_right)
        def _():
            line_piece(c, pc, q, 0).start()

        @pl.when(has_left)
        def _():
            line_piece(c, pc, q, 1).start()

    def own_w(c, pc):
        W[c][pc, h, p] = weights[pc][:, cols(p, c)]

    def collect(c, pc):
        for q in peers:
            slice_in(c, pc, q).wait_recv()
            push(c, pc, q)

    acts = (fwd, saved, cot)

    def act_out(j, i, q):
        return remote(acts[j].at[chunk(t)], X.at[j, p, chunk(t)], aS.at[j, i], aR.at[j, p], dev(q), t)

    def act_on(j):
        q, to = (over, near) if j == 1 else (near, over)
        there = X.at[j, q, chunk(t)]
        return remote(there, there, aS.at[j, 2], aR.at[j, q], dev(to), t)

    def act_in(j, q):
        there = X.at[j, q, chunk(t)]
        return remote(there, there, aS.at[j, 0], aR.at[j, q], dev(q), t)

    def act_share(j, i, q, o, m):
        there = X.at[j, q, chunk(t)]
        return remote(there, there, bS.at[j, i, o], bR.at[j, q, t], f, m)

    def act_shared(j, i, q, o, m):
        there = X.at[j, q, chunk(m)]
        return remote(there, there, bS.at[j, i, o], bR.at[j, q, m], f, m)

    def take(j, i):
        act_in(j, peers[i]).wait_recv()
        if i == (1 if j == 1 else 0):
            act_on(j).start()
        for o, m in enumerate(mates):
            act_share(j, i, peers[i], o, m).start()

    def relay(c, pc, s):
        @pl.when(h >= s)
        def _():
            line(c, pc, h - s, 0).wait_recv()

            @pl.when(has_right)
            def _():
                line(c, pc, h - s, 0).start()

        @pl.when(far >= s)
        def _():
            line(c, pc, h + s, 1).wait_recv()

            @pl.when(has_left)
            def _():
                line(c, pc, h + s, 1).start()

    def product(c, j, pc):
        return jnp.dot(
            X[j].reshape(tokens, D), W[c][pc].reshape(D, parts[c]), preferred_element_type=F32
        )

    def forward(c):
        positive = jnp.maximum(product(c, 0, 0), 0.0)
        H[c][0] = (positive * positive).astype(BF16)

    def backward(c):
        pre[c][...] = product(c, 1, 0)
        d_hidden = product(c, 2, 1)
        H[c][1] = (d_hidden * 2.0 * jnp.maximum(pre[c][...], 0.0)).astype(BF16)

    order = []
    for i in range((L + 1) // 2):
        order += [L - 1 - i] if L - 1 - i == i else [L - 1 - i, i]

    def to_right(c, d):
        return remote(G[c].at[d], from_left[c].at[d], gS.at[c, d], gL.at[c, d], right, t)

    def to_left(c, d):
        return remote(G[c].at[d], from_right[c].at[d], gS.at[c, d], gR.at[c, d], left, t)

    def grads(c):
        for d in order:
            term = lax.dot_general(
                X[1, :, :, d * deep:(d + 1) * deep].reshape(tokens, deep),
                H[c][1],
                (((0,), (0,)), ((), ())),
                preferred_element_type=F32,
            )
            G[c][d] = term.astype(BF16).reshape(B, Rw, parts[c])
            if d > 0:

                @pl.when(h == 0)
                def _():
                    to_right(c, d).start()

            if d < L - 1:

                @pl.when(far == 0)
                def _():
                    to_left(c, d).start()

    def add_left(c, d):
        remote(from_left[c].at[d], from_left[c].at[d], gS.at[c, d], gL.at[c, d], left, t).wait_recv()
        G[c][d] = (G[c][d].astype(F32) + from_left[c][d].astype(F32)).astype(BF16)

    def add_right(c, d):
        remote(from_right[c].at[d], from_right[c].at[d], gS.at[c, d], gR.at[c, d], right, t).wait_recv()
        G[c][d] = (G[c][d].astype(F32) + from_right[c][d].astype(F32)).astype(BF16)

    def grad_out(c, i, q):
        return remote(
            G[c].at[h, q], gout.at[:, cols(p, c)], hS.at[c, i], hR.at[c, p], dev(q), t
        )

    def sum_step(c, s):
        if s < L - 1:

            @pl.when(jnp.logical_and(has_left, h <= s))
            def _():
                add_left(c, far - s + 2 * h)
                to_right(c, far - s + 2 * h).start()

            @pl.when(jnp.logical_and(has_right, far <= s))
            def _():
                add_right(c, s - far)
                to_left(c, s - far).start()

        else:

            @pl.when(has_left)
            def _():
                add_left(c, h)

            @pl.when(has_right)
            def _():
                add_right(c, h)

            for i, q in enumerate(peers):
                grad_out(c, i, q).start()
            gout[:, cols(p, c)] = G[c][h, p]

    def columns(k):
        return pl.ds(pl.multiple_of(k * deep, deep), deep)

    def tp_out(o, i, m, k):
        return remote(
            O.at[o, :, chunk(m), columns(k)], tp_in.at[o, t, :, :, columns(k)],
            tS.at[o, i, k], tR.at[o, t, k], f, m,
        )

    def tp_got(o, i, m, k):
        there = tp_in.at[o, m, :, :, columns(k)]
        return remote(there, there, tS.at[o, i, k], tR.at[o, m, k], f, m)

    def by_near(o, k):
        return o == 0 or k % 2 == 0

    def first_out(o, k):
        src = S.at[o, :, 1 - b] if by_near(o, k) else S.at[o, 1 - a]
        return remote(
            src.at[:, :, columns(k)], near_in.at[o, :, :, columns(k)],
            nS.at[o, k], nR.at[o, k], dev(near if by_near(o, k) else over), t,
        )

    def second_out(o, k):
        src = S.at[o, 1 - a, b] if by_near(o, k) else S.at[o, a, 1 - b]
        return remote(
            src.at[:, columns(k)], far_in.at[o, :, columns(k)],
            mS.at[o, k], mR.at[o, k], dev(over if by_near(o, k) else near), t,
        )

    def spread(o, pc, k):
        part = 0.0
        for c in range(Q):
            block = W[c][pc, k].reshape(deep, parts[c])
            part += lax.dot_general(
                H[c][o], block, (((1,), (1,)), ((), ())), preferred_element_type=F32
            )
        O[o, :, :, columns(k)] = part.astype(BF16).reshape(B, rows, deep)
        for i, m in enumerate(mates):
            tp_out(o, i, m, k).start()

    def tp_sums(o, k):
        for i, m in enumerate(mates):
            tp_got(o, i, m, k).wait_recv()
        for first in (True, False):
            for other in range(2):
                if by_near(o, k):
                    aa, bb = other, 1 - b if first else b
                else:
                    aa, bb = 1 - a if first else a, other
                total = O[o, 2 * aa + bb, chunk(t), columns(k)].astype(F32)
                for m in mates:
                    total = total + tp_in[o, m, 2 * aa + bb, :, columns(k)].astype(F32)
                S[o, aa, bb, :, columns(k)] = total.astype(BF16)
            if first:
                first_out(o, k).start()

    def near_sums(o, k):
        first_out(o, k).wait_recv()
        for first in (True, False):
            if by_near(o, k):
                aa, bb = 1 - a if first else a, b
                got = aa
            else:
                aa, bb = a, 1 - b if first else b
                got = bb
            total = S[o, aa, bb, :, columns(k)].astype(F32) + near_in[o, got, :, columns(k)].astype(F32)
            S[o, aa, bb, :, columns(k)] = total.astype(BF16)
            if first:
                second_out(o, k).start()

    outs = (out, ing)

    def share(o, i, m):
        there = outs[o].at[chunk(t)]
        return remote(there, there, fS.at[o, i], fR.at[o, t], f, m)

    def shared(o, i, m):
        there = outs[o].at[chunk(m)]
        return remote(there, there, fS.at[o, i], fR.at[o, m], f, m)

    def finish(o):
        for k in range(K):
            second_out(o, k).wait_recv()
            total = S[o, a, b, :, columns(k)].astype(F32) + far_in[o, :, columns(k)].astype(F32)
            outs[o][chunk(t), columns(k)] = total.astype(BF16)
        for i, m in enumerate(mates):
            share(o, i, m).start()

    def slices(c):
        for pc in range(2):
            if (c, pc) == (0, 1) and weights[1] is turned:
                turned[...] = down[...].T
            for i, q in enumerate(peers):
                slice_out(c, pc, i, q).start()

    def pieces(c):
        for pc in range(2):
            push(c, pc, p)

    def keep_own():
        for c, pc in stages:
            own_w(c, pc)
        for j in range(3):
            X[j, p] = acts[j][...]

    def settle(j):
        for i, q in enumerate(peers):
            for o, m in enumerate(mates):
                act_shared(j, i, q, o, m).wait_recv()

    def some(work):
        def run(o, k):
            for part in range(k * K // 4, (k + 1) * K // 4):
                work(o, part)

        return run

    def reach(at, work):
        for s in range((at - 1) * (L - 1) // 3 + 1, at * (L - 1) // 3 + 1) if at else (0,):
            if s == 0:
                work(h)
                continue

            @pl.when(h >= s)
            def _():
                work(h - s)

            @pl.when(far >= s)
            def _():
                work(h + s)

    def steps(work):
        def run(*args):
            at = args[-1]
            for s in range((at - 1) * (L - 1) // 3, at * (L - 1) // 3):
                work(*args[:-1], s + 1)

        return run

    by_part = {
        "slices": slices, "pieces": pieces, "collect": collect, "relay": steps(relay), "sums": steps(sum_step),
        "forward": forward, "backward": backward, "grads": grads,
    }
    others = {
        "over": lambda j: act_out(j, 1, over).start(),
        "near": lambda j: act_out(j, 0, near).start(),
        "take": take, "settle": settle, "keep_own": keep_own, "finish": finish,
        "spread_at": lambda s: reach(s, lambda k: spread(0, 1, k)),
        "tp_at": lambda s: reach(s, lambda k: tp_sums(0, k)),
        "near_at": lambda s: reach(s, lambda k: near_sums(0, k)),
        "spread": some(lambda o, k: spread(o, 1 - o, k)),
        "tp_sums": some(tp_sums), "near_sums": some(near_sums),
    }
    for name, *args in SCHEDULE:
        if name in others:
            others[name](*args)
        elif args[0] < Q:
            by_part[name](*args)

    for i, q in enumerate(peers):
        for c in range(Q):
            there = gout.at[:, cols(q, c)]
            remote(there, there, hS.at[c, i], hR.at[c, q], dev(q), t).wait_recv()
            grad_out(c, i, q).wait_send()
            for pc in range(2):
                slice_out(c, pc, i, q).wait_send()
        for j in range(3):
            for o, m in enumerate(mates):
                act_share(j, i, q, o, m).wait_send()
    for j in range(3):
        act_out(j, 0, near).wait_send()
        act_out(j, 1, over).wait_send()
        act_on(j).wait_send()
    for o in range(2):
        for k in range(K):
            first_out(o, k).wait_send()
            second_out(o, k).wait_send()
        for i, m in enumerate(mates):
            for k in range(K):
                tp_out(o, i, m, k).wait_send()
            share(o, i, m).wait_send()
            shared(o, i, m).wait_recv()
    for c in range(Q):
        for k in range(L):
            @pl.when(h < k)
            def _(c=c, k=k):
                to_right(c, k).wait_send()

            @pl.when(h > k)
            def _(c=c, k=k):
                to_left(c, k).wait_send()

        for pc in range(2):
            for s in range(L):

                @pl.when(jnp.logical_and(has_right, h >= s))
                def _(c=c, pc=pc, s=s):
                    line(c, pc, h - s, 0).wait_send()

                @pl.when(jnp.logical_and(has_left, far >= s))
                def _(c=c, pc=pc, s=s):
                    line(c, pc, h + s, 1).wait_send()


def widths(whole):
    return PARTS if whole == sum(PARTS) else [whole]


def per_device(n, T, fwd_input, saved_input, out_cotangent, up_weight, down_weight, up_grad_sum):
    rows, D = fwd_input.shape
    Rw, F = up_weight.shape
    B = 4
    L, Fs, C = n // B, F // B, rows // T
    parts = widths(Fs)
    Q = len(parts)
    K = D // (B * Rw)
    down = down_weight if Rw % 128 == 0 and down_weight.shape != up_weight.shape else down_weight.T
    dma = pltpu.SemaphoreType.DMA
    mate = max(T - 1, 1)
    flops = 12 * B * rows * Fs * D
    vmem = pl.BlockSpec(memory_space=pltpu.VMEM)
    layer_out, input_grad, grad = pl.pallas_call(
        functools.partial(kernel, n, T, B, parts),
        out_shape=(
            jax.ShapeDtypeStruct((rows, D), BF16),
            jax.ShapeDtypeStruct((rows, D), BF16),
            jax.ShapeDtypeStruct((Rw, F), BF16),
        ),
        in_specs=[vmem] * 5,
        out_specs=(vmem,) * 3,
        scratch_shapes=[
            pltpu.VMEM((3, B, rows, D), BF16),
            pltpu.VMEM((Rw, F), BF16),
            pltpu.VMEM((2, B, rows, D), BF16),
            pltpu.VMEM((2, T, B, C, D), BF16),
            pltpu.VMEM((2, 2, 2, C, D), BF16),
            pltpu.VMEM((2, 2, C, D), BF16),
            pltpu.VMEM((2, C, D), BF16),
            [pltpu.VMEM((2, L, B, Rw, wide), BF16) for wide in parts],
            [pltpu.VMEM((2, B * rows, wide), BF16) for wide in parts],
            [pltpu.VMEM((B * rows, wide), F32) for wide in parts],
            [pltpu.VMEM((L, B, Rw, wide), BF16) for wide in parts],
            [pltpu.VMEM((L, B, Rw, wide), BF16) for wide in parts],
            [pltpu.VMEM((L, B, Rw, wide), BF16) for wide in parts],
            dma((Q, 2, 3)), dma((Q, 2, B)),
            dma((2, Q, 2, L)), dma((Q, 2, L)),
            dma((3, 3)), dma((3, B)),
            dma((3, 3, mate)), dma((3, B, T)),
            dma((2, mate, K)), dma((2, T, K)),
            dma((2, K)), dma((2, K)),
            dma((2, K)), dma((2, K)),
            dma((2, mate)), dma((2, T)),
            dma((Q, L)), dma((Q, L)), dma((Q, L)),
            dma((Q, 3)), dma((Q, B)),
        ],
        compiler_params=pltpu.CompilerParams(
            collective_id=0, has_side_effects=True, vmem_limit_bytes=58 * 2**20
        ),
        cost_estimate=pl.CostEstimate(flops=flops, bytes_accessed=2**25, transcendentals=0),
    )(fwd_input, saved_input, out_cotangent, up_weight, down)
    grad_part = grad.astype(F32)
    grad_scale = float(rows * n) ** (-0.5)
    return (layer_out, input_grad, up_grad_sum + grad_part * grad_scale)


def solution(mesh):
    placed = (
        P("fs", None),
        P("fs", None),
        P("fs", None),
        P("fs", "tp"),
        P("tp", "fs"),
        P("fs", "tp"),
    )
    return jax.shard_map(
        functools.partial(per_device, mesh.shape["fs"], mesh.shape["tp"]),
        mesh=mesh,
        in_specs=placed,
        out_specs=(P("fs", None), P("fs", None), P("fs", "tp")),
        check_vma=False,
    )
```

time: 123 us -> 114 us (0.927); the launches traced: 121 us -> 114 us
  Pallas kernels: 116 us -> 109 us
    pallas_call x1, Pallas kernels: 116 us -> 109 us  [per_device(): pl.pallas_call(functools.partial(kernel, n, T, B, parts), out_shape=(jax....]
where the time goes in v1:
time: 114 us
  Pallas kernels  109 us (96%)
  other arithmetic  2.2 us (2%)
  local copies, waits for them, and re-layouts  2.03 us (2%)
    pallas_call x1, Pallas kernels, per_device(): pl.pallas_call(functools.partial(kernel, n, T, B, parts), out_shape=(jax....  109 us

profile of v1, /device:TPU:0, one launch (start us, length us, event | category | flops | bytes accessed | tf_op | source)
XLA Modules:
  0.0 114.2 jit_solution(7775826457239445793)
XLA Ops:
  0.6 0.0 copy-start
  0.6 109.2 %shard_map.85 = (bf16[128,2048]{1,0:T(8,128)(2,1)}, bf16[128,2048]{1,0:T(8,128)(2,1)}, bf16[128,2048]{1,0:T(8,128)(2,1)}) custom-call(bf16[128,2048]{1,0:T(8,128)(2,1)} %fwd.1, bf16[128,2048]{1,0:T(8,128)(2,1)} %saved.1, bf16[128,2048]{1,0:T(8,128)(2,1)} %cot.1, bf16[128,2048]{1,0:T(8,128)(2,1)} %up.1, bf16[2048,128]{1,0:T(8,128)(2,1)} %down.1), custom_call_target="tpu_custom_call" | custom-call | flops 6442450944 | bytes 33554432 | tf_op jit(solution)/shard_map/pallas_call | solution.py:475
  109.9 0.0 copy-done
  109.9 0.0 copy-start.2
  109.9 2.2 %multiply_add_fusion = f32[128,2048]{1,0:T(8,128)} fusion(f32[128,2048]{1,0:T(8,128)S(1)} %copy-done, bf16[128,2048]{1,0:T(8,128)(2,1)} %get-tuple-element.8), kind=kLoop, calls=%fused_computation | loop fusion | flops 786432 | bytes 2621440 | tf_op jit(solution)/shard_map/add | solution.py:516
  112.1 0.0 copy-done.2
  112.1 0.0 copy-start.1
  112.1 0.8 copy.11
  112.9 0.4 copy-done.1
  113.4 0.8 copy.12
Async XLA Ops:
  0.6 109.3 %copy-start = (f32[128,2048]{1,0:T(8,128)S(1)}, f32[128,2048]{1,0:T(8,128)}, u32[]{:S(2)}) copy-start(f32[128,2048]{1,0:T(8,128)} %param.11) | copy-start | bytes 3145732
  109.9 2.2 %copy-start.2 = (bf16[128,2048]{1,0:T(8,128)(2,1)S(1)}, bf16[128,2048]{1,0:T(8,128)(2,1)}, u32[]{:S(2)}) copy-start(bf16[128,2048]{1,0:T(8,128)(2,1)} %get-tuple-element.12) | copy-start | bytes 1572868
  112.1 1.2 %copy-start.1 = (bf16[128,2048]{1,0:T(8,128)(2,1)S(1)}, bf16[128,2048]{1,0:T(8,128)(2,1)}, u32[]{:S(2)}) copy-start(bf16[128,2048]{1,0:T(8,128)(2,1)} %get-tuple-element.13) | copy-start | bytes 1572868

commit v2 on v1

--- a/solution.py
+++ b/solution.py
@@ -10,6 +10,7 @@
 MESH = pl.DeviceIdType.MESH
 F32 = jnp.float32
 BF16 = jnp.bfloat16
+SPLIT = 2
 PARTS = [256, 128, 128]
 SCHEDULE = [('slices', 0), ('pieces', 0), ('pieces', 1), ('slices', 1), ('slices', 2), ('collect', 0, 0), ('over', 1), ('collect', 0, 1), ('relay', 0, 0, 1), ('relay', 0, 1, 1), ('near', 1), ('near', 2), ('pieces', 2), ('near', 0), ('over', 2), ('over', 0), ('take', 2, 1), ('collect', 1, 0), ('relay', 0, 0, 2), ('relay', 0, 0, 3), ('take', 1, 0), ('take', 0, 1), ('relay', 0, 1, 2), ('collect', 1, 1), ('keep_own',), ('collect', 2, 0), ('take', 1, 1), ('collect', 2, 1), ('relay', 0, 1, 3), ('relay', 1, 0, 1), ('take', 2, 0), ('take', 1, 2), ('take', 2, 2), ('settle', 1), ('settle', 2), ('take', 0, 0), ('backward', 0), ('grads', 0), ('relay', 1, 0, 2), ('relay', 2, 0, 1), ('relay', 1, 0, 3), ('relay', 1, 1, 1), ('relay', 1, 1, 2), ('take', 0, 2), ('relay', 1, 1, 3), ('settle', 0), ('backward', 1), ('grads', 1), ('forward', 0), ('forward', 1), ('relay', 2, 0, 2), ('relay', 2, 0, 3), ('forward', 2), ('relay', 2, 1, 1), ('spread_at', 0), ('spread_at', 1), ('relay', 2, 1, 2), ('tp_at', 0), ('tp_at', 1), ('spread_at', 2), ('relay', 2, 1, 3), ('backward', 2), ('tp_at', 2), ('sums', 0, 1), ('sums', 0, 2), ('spread', 1, 0), ('spread', 1, 1), ('tp_sums', 1, 0), ('grads', 2), ('spread_at', 3), ('spread', 1, 2), ('tp_at', 3), ('tp_sums', 1, 1), ('near_at', 2), ('near_at', 0), ('sums', 1, 1), ('spread', 1, 3), ('tp_sums', 1, 3), ('near_at', 1), ('tp_sums', 1, 2), ('near_sums', 1, 1), ('sums', 1, 2), ('near_at', 3), ('near_sums', 1, 2), ('near_sums', 1, 0), ('sums', 2, 1), ('sums', 0, 3), ('near_sums', 1, 3), ('sums', 1, 3), ('sums', 2, 2), ('sums', 2, 3), ('finish', 0), ('finish', 1)]
 
@@ -281,12 +282,9 @@
         )
 
     def spread(o, pc, k):
-        part = 0.0
-        for c in range(Q):
-            block = W[c][pc, k].reshape(deep, parts[c])
-            part += lax.dot_general(
-                H[c][o], block, (((1,), (1,)), ((), ())), preferred_element_type=F32
-            )
+        units = jnp.concatenate([H[c][o] for c in range(Q)], axis=1)
+        block = jnp.concatenate([W[c][pc, k].reshape(deep, parts[c]) for c in range(Q)], axis=1)
+        part = lax.dot_general(units, block, (((1,), (1,)), ((), ())), preferred_element_type=F32)
         O[o, :, :, columns(k)] = part.astype(BF16).reshape(B, rows, deep)
         for i, m in enumerate(mates):
             tp_out(o, i, m, k).start()
@@ -453,6 +451,40 @@
                 @pl.when(jnp.logical_and(has_left, far >= s))
                 def _(c=c, pc=pc, s=s):
                     line(c, pc, h + s, 1).wait_send()
+
+
+def hand_over(scale, out, ing, grad, running, out_to, ing_to, grad_to, o, i, g, r, total, came, went):
+    def pieces(src, dst, sem):
+        size = src.shape[0] // SPLIT
+        return [
+            pltpu.make_async_copy(src.at[pl.ds(at * size, size)], dst.at[pl.ds(at * size, size)], sem.at[at])
+            for at in range(SPLIT)
+        ]
+
+    ins = [
+        pieces(src, dst, came.at[at])
+        for at, (src, dst) in enumerate(((running, r), (grad, g), (out, o), (ing, i)))
+    ]
+    outs = [
+        pieces(src, dst, went.at[at])
+        for at, (src, dst) in enumerate(((total, grad_to), (o, out_to), (i, ing_to)))
+    ]
+    for at in range(SPLIT):
+        for copies in ins:
+            copies[at].start()
+    size = total.shape[0] // SPLIT
+    for at in range(SPLIT):
+        part = pl.ds(at * size, size)
+        ins[0][at].wait()
+        ins[1][at].wait()
+        total[part] = r[part] + g[part].astype(F32) * scale
+        outs[0][at].start()
+        for copies in (1, 2):
+            ins[copies + 1][at].wait()
+            outs[copies][at].start()
+    for copies in outs:
+        for copy in copies:
+            copy.wait()
 
 
 def widths(whole):
@@ -511,9 +543,27 @@
         ),
         cost_estimate=pl.CostEstimate(flops=flops, bytes_accessed=2**25, transcendentals=0),
     )(fwd_input, saved_input, out_cotangent, up_weight, down)
-    grad_part = grad.astype(F32)
     grad_scale = float(rows * n) ** (-0.5)
-    return (layer_out, input_grad, up_grad_sum + grad_part * grad_scale)
+    anywhere = pl.BlockSpec(memory_space=pl.ANY)
+    return pl.pallas_call(
+        functools.partial(hand_over, grad_scale),
+        out_shape=(
+            jax.ShapeDtypeStruct((rows, D), BF16),
+            jax.ShapeDtypeStruct((rows, D), BF16),
+            jax.ShapeDtypeStruct((Rw, F), F32),
+        ),
+        in_specs=[anywhere] * 4,
+        out_specs=(anywhere,) * 3,
+        scratch_shapes=[
+            pltpu.VMEM((rows, D), BF16),
+            pltpu.VMEM((rows, D), BF16),
+            pltpu.VMEM((Rw, F), BF16),
+            pltpu.VMEM((Rw, F), F32),
+            pltpu.VMEM((Rw, F), F32),
+            dma((4, SPLIT)), dma((3, SPLIT)),
+        ],
+        cost_estimate=pl.CostEstimate(flops=2 * Rw * F, bytes_accessed=14 * Rw * F, transcendentals=0),
+    )(layer_out, input_grad, grad, up_grad_sum)
 
 
 def solution(mesh):

time: 114 us -> 112 us (0.982)
  other arithmetic: 2.2 us -> 0 us
  local copies, waits for them, and re-layouts: 2.03 us -> 0 us
  Pallas kernels: 109 us -> 111 us
    pallas_call x0 -> x1, Pallas kernels: none -> 2.64 us  [per_device(): pl.pallas_call(functools.partial(hand_over, grad_scale), out_shape=(jax.S...]
    add x1 -> x0, other arithmetic: 2.2 us -> none  [per_device(): return (layer_out, input_grad, up_grad_sum + grad_part * grad_scale)]
    unnamed x8 -> x0, local copies, waits for them, and re-layouts: 2.03 us -> none
where the time goes in v2:
time: 112 us
  Pallas kernels  111 us (99%)
    pallas_call x1, Pallas kernels, per_device(): pl.pallas_call(functools.partial(kernel, n, T, B, parts), out_shape=(jax....  109 us
    pallas_call x1, Pallas kernels, per_device(): pl.pallas_call(functools.partial(hand_over, grad_scale), out_shape=(jax.S...  2.64 us

profile of v2, /device:TPU:0, one launch (start us, length us, event | category | flops | bytes accessed | tf_op | source)
XLA Modules:
  0.0 112.0 jit_solution(11031410908489448347)
XLA Ops:
  0.6 108.6 %shard_map.85 = (bf16[128,2048]{1,0:T(8,128)(2,1)}, bf16[128,2048]{1,0:T(8,128)(2,1)}, bf16[128,2048]{1,0:T(8,128)(2,1)}) custom-call(bf16[128,2048]{1,0:T(8,128)(2,1)} %fwd.1, bf16[128,2048]{1,0:T(8,128)(2,1)} %saved.1, bf16[128,2048]{1,0:T(8,128)(2,1)} %cot.1, bf16[128,2048]{1,0:T(8,128)(2,1)} %up.1, bf16[2048,128]{1,0:T(8,128)(2,1)} %down.1), custom_call_target="tpu_custom_call" | custom-call | flops 6442450944 | bytes 33554432 | tf_op jit(solution)/shard_map/pallas_call | solution.py:507
  109.2 2.6 %shard_map.86 = (bf16[128,2048]{1,0:T(8,128)(2,1)}, bf16[128,2048]{1,0:T(8,128)(2,1)}, f32[128,2048]{1,0:T(8,128)}) custom-call(bf16[128,2048]{1,0:T(8,128)(2,1)} %get-tuple-element.6.out, bf16[128,2048]{1,0:T(8,128)(2,1)} %get-tuple-element.7.ing, bf16[128,2048]{1,0:T(8,128)(2,1)} %get-tuple-element.8.grad, f32[128,2048]{1,0:T(8,128)} %running.1), custom_call_target="tpu_custom_call" | custom-call | flops 524288 | bytes 3670016 | tf_op jit(solution)/shard_map/pallas_call | solution.py:548

commit v3 on v2

--- a/solution.py
+++ b/solution.py
@@ -12,7 +12,7 @@
 BF16 = jnp.bfloat16
 SPLIT = 2
 PARTS = [256, 128, 128]
-SCHEDULE = [('slices', 0), ('pieces', 0), ('pieces', 1), ('slices', 1), ('slices', 2), ('collect', 0, 0), ('over', 1), ('collect', 0, 1), ('relay', 0, 0, 1), ('relay', 0, 1, 1), ('near', 1), ('near', 2), ('pieces', 2), ('near', 0), ('over', 2), ('over', 0), ('take', 2, 1), ('collect', 1, 0), ('relay', 0, 0, 2), ('relay', 0, 0, 3), ('take', 1, 0), ('take', 0, 1), ('relay', 0, 1, 2), ('collect', 1, 1), ('keep_own',), ('collect', 2, 0), ('take', 1, 1), ('collect', 2, 1), ('relay', 0, 1, 3), ('relay', 1, 0, 1), ('take', 2, 0), ('take', 1, 2), ('take', 2, 2), ('settle', 1), ('settle', 2), ('take', 0, 0), ('backward', 0), ('grads', 0), ('relay', 1, 0, 2), ('relay', 2, 0, 1), ('relay', 1, 0, 3), ('relay', 1, 1, 1), ('relay', 1, 1, 2), ('take', 0, 2), ('relay', 1, 1, 3), ('settle', 0), ('backward', 1), ('grads', 1), ('forward', 0), ('forward', 1), ('relay', 2, 0, 2), ('relay', 2, 0, 3), ('forward', 2), ('relay', 2, 1, 1), ('spread_at', 0), ('spread_at', 1), ('relay', 2, 1, 2), ('tp_at', 0), ('tp_at', 1), ('spread_at', 2), ('relay', 2, 1, 3), ('backward', 2), ('tp_at', 2), ('sums', 0, 1), ('sums', 0, 2), ('spread', 1, 0), ('spread', 1, 1), ('tp_sums', 1, 0), ('grads', 2), ('spread_at', 3), ('spread', 1, 2), ('tp_at', 3), ('tp_sums', 1, 1), ('near_at', 2), ('near_at', 0), ('sums', 1, 1), ('spread', 1, 3), ('tp_sums', 1, 3), ('near_at', 1), ('tp_sums', 1, 2), ('near_sums', 1, 1), ('sums', 1, 2), ('near_at', 3), ('near_sums', 1, 2), ('near_sums', 1, 0), ('sums', 2, 1), ('sums', 0, 3), ('near_sums', 1, 3), ('sums', 1, 3), ('sums', 2, 2), ('sums', 2, 3), ('finish', 0), ('finish', 1)]
+SCHEDULE = [('slices', 0), ('keep_own',), ('pieces', 0), ('near', 2), ('slices', 1), ('pieces', 1), ('collect', 0, 0), ('over', 1), ('collect', 0, 1), ('relay', 0, 0, 1), ('relay', 0, 1, 1), ('over', 0), ('near', 1), ('relay', 0, 0, 2), ('collect', 1, 0), ('slices', 2), ('relay', 0, 1, 2), ('over', 2), ('collect', 1, 1), ('take', 1, 1), ('relay', 0, 0, 3), ('pieces', 2), ('near', 0), ('collect', 2, 1), ('take', 1, 0), ('take', 2, 1), ('take', 2, 0), ('relay', 1, 0, 1), ('relay', 0, 1, 3), ('take', 2, 2), ('take', 1, 2), ('take', 0, 0), ('settle', 1), ('settle', 2), ('collect', 2, 0), ('relay', 1, 0, 2), ('relay', 1, 1, 1), ('take', 0, 1), ('backward', 0), ('grads', 0), ('take', 0, 2), ('relay', 1, 1, 2), ('relay', 1, 0, 3), ('settle', 0), ('relay', 2, 0, 1), ('forward', 0), ('relay', 1, 1, 3), ('backward', 1), ('grads', 1), ('relay', 2, 0, 2), ('forward', 1), ('relay', 2, 0, 3), ('forward', 2), ('relay', 2, 1, 1), ('spread_at', 0), ('spread_at', 1), ('tp_at', 0), ('tp_at', 1), ('relay', 2, 1, 2), ('spread_at', 2), ('tp_at', 2), ('relay', 2, 1, 3), ('spread_at', 3), ('sums', 0, 1), ('backward', 2), ('spread', 1, 0), ('spread', 1, 3), ('spread', 1, 1), ('tp_sums', 1, 0), ('near_at', 0), ('sums', 1, 1), ('tp_sums', 1, 1), ('tp_at', 3), ('grads', 2), ('spread', 1, 2), ('near_at', 2), ('tp_sums', 1, 3), ('sums', 0, 2), ('sums', 2, 1), ('sums', 1, 2), ('near_sums', 1, 0), ('tp_sums', 1, 2), ('sums', 0, 3), ('near_at', 3), ('near_sums', 1, 1), ('near_sums', 1, 2), ('near_at', 1), ('sums', 2, 2), ('near_sums', 1, 3), ('sums', 1, 3), ('finish', 0), ('sums', 2, 3), ('finish', 1)]
 
 
 def remote(src, dst, send_sem, recv_sem, fs, tp):

time: 112 us -> 111 us (level)
    pallas_call x1, Pallas kernels: 109 us -> 107 us  [per_device(): pl.pallas_call(functools.partial(kernel, n, T, B, parts), out_shape=(jax....]
where the time goes in v3:
time: 111 us; the launch traced here: 110 us
  Pallas kernels  110 us (99%)
    pallas_call x1, Pallas kernels, per_device(): pl.pallas_call(functools.partial(kernel, n, T, B, parts), out_shape=(jax....  107 us
    pallas_call x1, Pallas kernels, per_device(): pl.pallas_call(functools.partial(hand_over, grad_scale), out_shape=(jax.S...  2.64 us

profile of v3, /device:TPU:0, one launch (start us, length us, event | category | flops | bytes accessed | tf_op | source)
XLA Modules:
  0.0 110.4 jit_solution(8157184055874477586)
XLA Ops:
  0.6 107.0 %shard_map.85 = (bf16[128,2048]{1,0:T(8,128)(2,1)}, bf16[128,2048]{1,0:T(8,128)(2,1)}, bf16[128,2048]{1,0:T(8,128)(2,1)}) custom-call(bf16[128,2048]{1,0:T(8,128)(2,1)} %fwd.1, bf16[128,2048]{1,0:T(8,128)(2,1)} %saved.1, bf16[128,2048]{1,0:T(8,128)(2,1)} %cot.1, bf16[128,2048]{1,0:T(8,128)(2,1)} %up.1, bf16[2048,128]{1,0:T(8,128)(2,1)} %down.1), custom_call_target="tpu_custom_call" | custom-call | flops 6442450944 | bytes 33554432 | tf_op jit(solution)/shard_map/pallas_call | solution.py:507
  107.6 2.6 %shard_map.86 = (bf16[128,2048]{1,0:T(8,128)(2,1)}, bf16[128,2048]{1,0:T(8,128)(2,1)}, f32[128,2048]{1,0:T(8,128)}) custom-call(bf16[128,2048]{1,0:T(8,128)(2,1)} %get-tuple-element.6.out, bf16[128,2048]{1,0:T(8,128)(2,1)} %get-tuple-element.7.ing, bf16[128,2048]{1,0:T(8,128)(2,1)} %get-tuple-element.8.grad, f32[128,2048]{1,0:T(8,128)} %running.1), custom_call_target="tpu_custom_call" | custom-call | flops 524288 | bytes 3670016 | tf_op jit(solution)/shard_map/pallas_call | solution.py:548
